TPU v7x, 32 devices: a whole 2x2x4 slice. The times are simulated.
32 devices in a mesh: sp: 4 (over y, core), dp: 8 (over z, x).
Axes of the slice: x: 2, y: 2, z: 4, core: 2. Of those that a mesh axis runs over, the one named last changes fastest.
Arguments:
- query_rows: bfloat16 [8, 512, 4, 128], P('dp', 'sp'), may hold values from -6 to 6
- key_rows: bfloat16 [8, 512, 4, 128], P('dp', 'sp'), may hold values from -6 to 6
- value_rows: bfloat16 [8, 512, 4, 128], P('dp', 'sp'), may hold values from -6 to 6
- map_weight: float32 [4], P('sp'), may hold values from 0.3 to 0.8
- head_gain: float32 [128], replicated, may hold values from 0.1 to 1.9
Outputs:
- mixed: bfloat16 [8, 512, 4, 128], P('dp', 'sp')
All inputs are finite; a program needn't handle non-finite values.
Results may differ from a plain program's by a relative error of at most 0.0049.
Values may be sent and summed in bfloat16 or wider, within the bound.
A program may use at most 64 MiB of HBM per device.

v0:
```python
import math
import jax
import jax.numpy as jnp
from jax import lax
from jax.sharding import PartitionSpec as P

QK = 64
SEGMENT = 64


def map_output(query_map, key_map, value_head):
    length = key_map.shape[0]
    block_len = math.gcd(length, 512)
    key_segment = jnp.arange(length, dtype=jnp.int32) // SEGMENT

    def one_block(start):
        query_block = lax.dynamic_slice_in_dim(query_map, start, block_len, 0)
        query_segment = (start + jnp.arange(block_len, dtype=jnp.int32)) // SEGMENT
        visible = key_segment[None, :] <= query_segment[:, None]
        scores = jnp.dot(query_block, key_map.T, preferred_element_type=jnp.float32) * QK ** (-0.5)
        scores = jnp.where(visible, scores, -jnp.inf)
        scores = scores - jnp.max(scores, axis=-1, keepdims=True)
        raised = jnp.exp(scores)
        weights = raised / jnp.sum(raised, axis=-1, keepdims=True)
        return jnp.dot(weights.astype(jnp.bfloat16), value_head, preferred_element_type=jnp.float32)

    starts = jnp.arange(length // block_len, dtype=jnp.int32) * block_len
    return lax.map(one_block, starts).reshape(length, value_head.shape[1])


def per_heads(query_local, key_local, value_local):
    return lax.map(
        lambda group: map_output(group[0], group[1], group[2]),
        (
            query_local[0].transpose(1, 0, 2),
            key_local[0].transpose(1, 0, 2),
            value_local[0].transpose(1, 0, 2),
        ),
    )


def finish(first_part, second_part, map_weight, head_gain):
    attended = first_part - map_weight[:, None, None] * second_part
    mean_square = jnp.mean(attended * attended, axis=-1, keepdims=True)
    normed = (attended * lax.rsqrt(mean_square + 1e-06) * head_gain).astype(jnp.bfloat16)
    return normed.transpose(1, 0, 2)[None]


def on_device(query_rows, key_rows, value_rows, map_weight, head_gain):
    query_local, key_local, value_local = (
        lax.all_to_all(query_rows, "sp", split_axis=2, concat_axis=1, tiled=True),
        lax.all_to_all(key_rows, "sp", split_axis=2, concat_axis=1, tiled=True),
        lax.all_to_all(value_rows, "sp", split_axis=2, concat_axis=1, tiled=True),
    )
    first_part = per_heads(query_local[..., :QK], key_local[..., :QK], value_local)
    second_part = per_heads(query_local[..., QK:], key_local[..., QK:], value_local)
    normed = finish(first_part, second_part, map_weight, head_gain)
    return lax.all_to_all(normed, "sp", split_axis=1, concat_axis=2, tiled=True)


def solution(mesh):
    return jax.shard_map(
        on_device,
        mesh=mesh,
        in_specs=(
            P("dp", "sp", None, None),
            P("dp", "sp", None, None),
            P("dp", "sp", None, None),
            P("sp"),
            P(),
        ),
        out_specs=P("dp", "sp", None, None),
        check_vma=False,
    )
```

profile of v0, /device:TPU:0, one launch (start us, length us, event | category | flops | bytes accessed | tf_op | source)
XLA Modules:
  0.0 37.9 jit_solution(136135858623358631)
XLA Ops:
  0.0 1.6 %copy.24 = bf16[1,128,4,128]{3,1,0,2:T(8,128)(2,1)} copy(bf16[1,128,4,128]{3,2,1,0:T(4,128)(2,1)} %param.5) | data formatting | bytes 262144 | tf_op args[0]
  1.6 0.0 copy-start
  1.6 4.4 %all-to-all-start = ((bf16[1,128,4,128]{3,1,0,2:T(8,128)(2,1)}), bf16[1,128,4,128]{3,1,0,2:T(8,128)(2,1)S(1)}, u32[]{:S(2)}, u32[]{:S(2)}) async-start(bf16[1,128,4,128]{3,1,0,2:T(8,128)(2,1)} %copy.24), calls=%async_computation | async-start | bytes 262144 | tf_op jit(solution)/shard_map/all_to_all | solution.py:51
  6.0 0.0 copy-done
  6.0 0.0 copy-start.1
  6.0 0.7 %copy.26 = bf16[1,128,4,128]{3,1,0,2:T(8,128)(2,1)} copy(bf16[1,128,4,128]{3,2,1,0:T(4,128)(2,1)S(1)} %copy-done) | data formatting | bytes 262144 | tf_op args[1]
  6.6 0.3 copy-done.1
  6.9 0.7 %copy.28 = bf16[1,128,4,128]{3,1,0,2:T(8,128)(2,1)} copy(bf16[1,128,4,128]{3,2,1,0:T(4,128)(2,1)S(1)} %copy-done.1) | data formatting | bytes 262144 | tf_op args[2]
  8.3 2.3 %all-to-all-done = bf16[1,128,4,128]{3,1,0,2:T(8,128)(2,1)S(1)} async-done(((bf16[1,128,4,128]{3,1,0,2:T(8,128)(2,1)}), bf16[1,128,4,128]{3,1,0,2:T(8,128)(2,1)S(1)}, u32[]{:S(2)}, u32[]{:S(2)}) %all-to-all-start) | async-done | bytes 131104 | tf_op jit(solution)/shard_map/all_to_all | solution.py:51
  10.6 3.3 %all-to-all-start.1 = ((bf16[1,128,4,128]{3,1,0,2:T(8,128)(2,1)}), bf16[1,128,4,128]{3,1,0,2:T(8,128)(2,1)S(1)}, u32[]{:S(2)}, u32[]{:S(2)}) async-start(bf16[1,128,4,128]{3,1,0,2:T(8,128)(2,1)} %copy.26), calls=%async_computation.1 | async-start | bytes 262144 | tf_op jit(solution)/shard_map/all_to_all | solution.py:52
  13.9 4.6 %all-to-all-done.1 = bf16[1,128,4,128]{3,1,0,2:T(8,128)(2,1)S(1)} async-done(((bf16[1,128,4,128]{3,1,0,2:T(8,128)(2,1)}), bf16[1,128,4,128]{3,1,0,2:T(8,128)(2,1)S(1)}, u32[]{:S(2)}, u32[]{:S(2)}) %all-to-all-start.1) | async-done | bytes 131104 | tf_op jit(solution)/shard_map/all_to_all | solution.py:52
  18.5 3.3 %all-to-all-start.2 = ((bf16[1,128,4,128]{3,1,0,2:T(8,128)(2,1)}), bf16[1,128,4,128]{3,1,0,2:T(8,128)(2,1)S(1)}, u32[]{:S(2)}, u32[]{:S(2)}) async-start(bf16[1,128,4,128]{3,1,0,2:T(8,128)(2,1)} %copy.28), calls=%async_computation.2 | async-start | bytes 262144 | tf_op jit(solution)/shard_map/all_to_all | solution.py:53
  21.8 0.4 %fusion.8 = (f32[512]{0:T(512)S(1)}, f32[512,512]{0,1:T(8,128)S(1)}) fusion(bf16[1,512,1,128]{3,1,2,0:T(8,128)(2,1)S(1)} %bitcast.59, bf16[1,512,1,128]{3,1,2,0:T(8,128)(2,1)S(1)} %bitcast.55, s32[512]{0:T(512)S(1)} %add_select_fusion), kind=kOutput, calls=%fused_computation.27 | convolution fusion | flops 34602496 | bytes 1316864 | tf_op jit(solution)/shard_map/while/body/eval_jaxpr/while/body/eval_jaxpr/dot_general | solution.py:20
  22.2 0.3 fusion.9
  22.5 0.2 fusion.3
  22.7 0.2 fusion.2
  22.9 3.5 %all-to-all-done.2 = bf16[1,128,4,128]{3,1,0,2:T(8,128)(2,1)S(1)} async-done(((bf16[1,128,4,128]{3,1,0,2:T(8,128)(2,1)}), bf16[1,128,4,128]{3,1,0,2:T(8,128)(2,1)S(1)}, u32[]{:S(2)}, u32[]{:S(2)}) %all-to-all-start.2) | async-done | bytes 131104 | tf_op jit(solution)/shard_map/all_to_all | solution.py:53
  26.4 0.3 convolution_multiply_fusion.2
  26.7 0.4 multiply_reduce_fusion
  27.1 0.0 copy-start.2
  27.1 0.6 %copy-done.2 = f32[128]{0:T(128)S(1)} copy-done((f32[128]{0:T(128)S(1)}, f32[128]{0:T(128)}, u32[]{:S(2)}) %copy-start.2) | copy-done | bytes 536
  27.8 0.1 fusion.4
  27.8 0.2 copy.31
  28.0 0.5 %broadcast.100 = bf16[]{:T(256)} broadcast(bf16[]{:T(256)} %constant.139), dimensions={} | broadcast | bytes 4
  28.5 1.4 %reduce.2 = bf16[512,128]{1,0:T(8,128)(2,1)S(1)} reduce(bf16[512,1,1,128]{3,2,1,0:T(2,128)(2,1)S(1)} %bitcast.52, bf16[]{:T(256)} %broadcast.100), dimensions={1,2}, to_apply=%bitcast.39.reduce_sub_computation | reduce | bytes 262146
  30.0 7.0 %all_to_all.69 = bf16[4,2,8192]{2,1,0:T(2,128)(2,1)S(1)} all-to-all(bf16[4,2,8192]{2,1,0:T(2,128)(2,1)S(1)} %reshape.64), channel_id=1, replica_groups=mesh['sp'=4,'dp'=8] {'sp'}, dimensions={0} | all-to-all | bytes 262144 | tf_op jit(solution)/shard_map/all_to_all | solution.py:58
  37.0 0.1 reshape.65
  37.1 0.8 %copy.32 = bf16[1,128,4,128]{3,2,1,0:T(4,128)(2,1)} copy(bf16[1,128,4,128]{3,1,2,0:T(8,128)(2,1)S(1)} %bitcast.54) | data formatting | bytes 262144 | tf_op jit(solution)/shard_map/all_to_all | solution.py:58
  (4 shorter events, 0.1 us)
Async XLA Ops:
  1.6 4.4 %copy-start = (bf16[1,128,4,128]{3,2,1,0:T(4,128)(2,1)S(1)}, bf16[1,128,4,128]{3,2,1,0:T(4,128)(2,1)}, u32[]{:S(2)}) copy-start(bf16[1,128,4,128]{3,2,1,0:T(4,128)(2,1)} %param.6) | copy-start | bytes 393220
  1.6 9.0 %all-to-all-start = ((bf16[1,128,4,128]{3,1,0,2:T(8,128)(2,1)}), bf16[1,128,4,128]{3,1,0,2:T(8,128)(2,1)S(1)}, u32[]{:S(2)}, u32[]{:S(2)}) async-start(bf16[1,128,4,128]{3,1,0,2:T(8,128)(2,1)} %copy.24), calls=%async_computation | async-start | bytes 262144 | tf_op jit(solution)/shard_map/all_to_all | solution.py:51
  6.0 1.0 %copy-start.1 = (bf16[1,128,4,128]{3,2,1,0:T(4,128)(2,1)S(1)}, bf16[1,128,4,128]{3,2,1,0:T(4,128)(2,1)}, u32[]{:S(2)}) copy-start(bf16[1,128,4,128]{3,2,1,0:T(4,128)(2,1)} %param.7) | copy-start | bytes 393220
  10.6 7.9 %all-to-all-start.1 = ((bf16[1,128,4,128]{3,1,0,2:T(8,128)(2,1)}), bf16[1,128,4,128]{3,1,0,2:T(8,128)(2,1)S(1)}, u32[]{:S(2)}, u32[]{:S(2)}) async-start(bf16[1,128,4,128]{3,1,0,2:T(8,128)(2,1)} %copy.26), calls=%async_computation.1 | async-start | bytes 262144 | tf_op jit(solution)/shard_map/all_to_all | solution.py:52
  18.5 7.9 %all-to-all-start.2 = ((bf16[1,128,4,128]{3,1,0,2:T(8,128)(2,1)}), bf16[1,128,4,128]{3,1,0,2:T(8,128)(2,1)S(1)}, u32[]{:S(2)}, u32[]{:S(2)}) async-start(bf16[1,128,4,128]{3,1,0,2:T(8,128)(2,1)} %copy.28), calls=%async_computation.2 | async-start | bytes 262144 | tf_op jit(solution)/shard_map/all_to_all | solution.py:53
  27.1 0.7 %copy-start.2 = (f32[128]{0:T(128)S(1)}, f32[128]{0:T(128)}, u32[]{:S(2)}) copy-start(f32[128]{0:T(128)} %param.9) | copy-start | bytes 1540
where the time goes:
time: 38.4 us; the launch traced here: 37.9 us
  starting transfers between devices  11 us (29%)
  waiting for transfers between devices  10.3 us (27%)
  blocking collectives  6.99 us (18%)
  local copies, waits for them, and re-layouts  5.47 us (14%)
  other arithmetic  1.89 us (5%)
  matrix products  1.41 us (4%)
  between operations  0.75 us (2%)
    all_to_all x1, blocking collectives, on_device(): return lax.all_to_all(normed, 'sp', split_axis=1, concat_axis=2, tiled=True)  6.99 us
    all_to_all x1, waiting for transfers between devices, on_device(): lax.all_to_all(key_rows, 'sp', split_axis=2, concat_axis=1, tiled=True)  4.56 us
    unnamed x13, local copies, waits for them, and re-layouts  4.55 us
    all_to_all x1, starting transfers between devices, on_device(): lax.all_to_all(query_rows, 'sp', split_axis=2, concat_axis=1, tiled=True)  4.4 us
    all_to_all x1, waiting for transfers between devices, on_device(): lax.all_to_all(value_rows, 'sp', split_axis=2, concat_axis=1, tiled=True)  3.45 us
    all_to_all x1, starting transfers between devices, on_device(): lax.all_to_all(value_rows, 'sp', split_axis=2, concat_axis=1, tiled=True)  3.33 us
    all_to_all x1, starting transfers between devices, on_device(): lax.all_to_all(key_rows, 'sp', split_axis=2, concat_axis=1, tiled=True)  3.32 us
    all_to_all x1, waiting for transfers between devices, on_device(): lax.all_to_all(query_rows, 'sp', split_axis=2, concat_axis=1, tiled=True)  2.32 us
  transfers between devices with their start and end apart: 3, of which 3 were waited for; matrix products, arithmetic and copies ran while one was open for 6% of the time, Pallas kernels for 0%

commit v1 on v0

--- a/solution.py
+++ b/solution.py
@@ -6,6 +6,12 @@
 
 QK = 64
 SEGMENT = 64
+
+
+def trade_parts(x, name, split, join):
+    pieces = jnp.split(x, lax.axis_size(name), axis=split)
+    arrived = lax.all_to_all(jnp.stack(pieces), name, 0, 0)
+    return jnp.concatenate(arrived, axis=join)
 
 
 def map_output(query_map, key_map, value_head):
@@ -50,7 +56,7 @@
     query_local, key_local, value_local = (
         lax.all_to_all(query_rows, "sp", split_axis=2, concat_axis=1, tiled=True),
         lax.all_to_all(key_rows, "sp", split_axis=2, concat_axis=1, tiled=True),
-        lax.all_to_all(value_rows, "sp", split_axis=2, concat_axis=1, tiled=True),
+        trade_parts(value_rows, "sp", 2, 1),
     )
     first_part = per_heads(query_local[..., :QK], key_local[..., :QK], value_local)
     second_part = per_heads(query_local[..., QK:], key_local[..., QK:], value_local)

time: 38.4 us -> 38.4 us (level)
  other arithmetic: 1.89 us -> 2.57 us
  waiting for transfers between devices: 10.3 us -> 9.68 us
    another operation x0 -> x1, other arithmetic: none -> 0.68 us  [trade_parts(): arrived = lax.all_to_all(jnp.stack(pieces), name, 0, 0)]
    all_to_all x1, waiting for transfers between devices: 2.32 us -> 1.67 us  [on_device(): lax.all_to_all(query_rows, 'sp', split_axis=2, concat_axis=1, tiled=True)]
    unnamed x13 -> x12, local copies, waits for them, and re-layouts: 4.55 us -> 4.29 us
  transfers between devices with their start and end apart: 3 -> 3, of which waited for: 3 -> 3; matrix products, arithmetic and copies ran while one was open for 6% -> 7% of each run, Pallas kernels for 0% -> 0%
where the time goes in v1:
time: 38.4 us; the launch traced here: 37.9 us
  starting transfers between devices  11 us (29%)
  waiting for transfers between devices  9.68 us (25%)
  blocking collectives  6.99 us (18%)
  local copies, waits for them, and re-layouts  5.42 us (14%)
  other arithmetic  2.57 us (7%)
  matrix products  1.41 us (4%)
  between operations  0.77 us (2%)
    all_to_all x1, blocking collectives, on_device(): return lax.all_to_all(normed, 'sp', split_axis=1, concat_axis=2, tiled=True)  6.99 us
    all_to_all x1, waiting for transfers between devices, on_device(): lax.all_to_all(key_rows, 'sp', split_axis=2, concat_axis=1, tiled=True)  4.56 us
    all_to_all x1, starting transfers between devices, on_device(): lax.all_to_all(query_rows, 'sp', split_axis=2, concat_axis=1, tiled=True)  4.4 us
    unnamed x12, local copies, waits for them, and re-layouts  4.29 us
    all_to_all x1, waiting for transfers between devices, trade_parts(): arrived = lax.all_to_all(jnp.stack(pieces), name, 0, 0)  3.45 us
    all_to_all x1, starting transfers between devices, trade_parts(): arrived = lax.all_to_all(jnp.stack(pieces), name, 0, 0)  3.33 us
    all_to_all x1, starting transfers between devices, on_device(): lax.all_to_all(key_rows, 'sp', split_axis=2, concat_axis=1, tiled=True)  3.32 us
    all_to_all x1, waiting for transfers between devices, on_device(): lax.all_to_all(query_rows, 'sp', split_axis=2, concat_axis=1, tiled=True)  1.67 us
  transfers between devices with their start and end apart: 3, of which 3 were waited for; matrix products, arithmetic and copies ran while one was open for 7% of the time, Pallas kernels for 0%

profile of v1, /device:TPU:0, one launch (start us, length us, event | category | flops | bytes accessed | tf_op | source)
XLA Modules:
  0.0 37.9 jit_solution(7622704867988350492)
XLA Ops:
  0.0 1.6 %copy.33 = bf16[1,128,4,128]{3,1,0,2:T(8,128)(2,1)} copy(bf16[1,128,4,128]{3,2,1,0:T(4,128)(2,1)} %param.5) | data formatting | bytes 262144 | tf_op args[0]
  1.6 0.0 copy-start
  1.6 4.4 %all-to-all-start = ((bf16[1,128,4,128]{3,1,0,2:T(8,128)(2,1)}), bf16[1,128,4,128]{3,1,0,2:T(8,128)(2,1)S(1)}, u32[]{:S(2)}, u32[]{:S(2)}) async-start(bf16[1,128,4,128]{3,1,0,2:T(8,128)(2,1)} %copy.33), calls=%async_computation | async-start | bytes 262144 | tf_op jit(solution)/shard_map/all_to_all | solution.py:57
  6.0 0.0 copy-done
  6.0 0.0 copy-start.1
  6.0 0.2 fusion.8
  6.2 0.7 %copy-done.1 = bf16[1,128,4,128]{3,2,1,0:T(4,128)(2,1)S(1)} copy-done((bf16[1,128,4,128]{3,2,1,0:T(4,128)(2,1)S(1)}, bf16[1,128,4,128]{3,2,1,0:T(4,128)(2,1)}, u32[]{:S(2)}) %copy-start.1) | copy-done | bytes 131096
  6.9 0.7 %copy.35 = bf16[1,128,4,128]{3,1,0,2:T(8,128)(2,1)} copy(bf16[1,128,4,128]{3,2,1,0:T(4,128)(2,1)S(1)} %copy-done.1) | data formatting | bytes 262144 | tf_op args[1]
  8.2 0.7 %pad_maximum_fusion = bf16[4,1,128,1,128]{4,2,3,1,0:T(8,128)(2,1)} fusion(bf16[1,1,128,1,128]{4,2,3,1,0:T(8,128)(2,1)S(1)} %get-tuple-element.93, bf16[1,1,128,1,128]{4,2,3,1,0:T(8,128)(2,1)S(1)} %get-tuple-element.94, bf16[1,1,128,1,128]{4,2,3,1,0:T(8,128)(2,1)S(1)} %get-tuple-element.95, bf16[1,1,128,1,128]{4,2,3,1,0:T(8,128)(2,1)S(1)} %get-tuple-element.96), kind=kLoop, calls=%fused_computation.19 | loop fusion | flops 196608 | bytes 262144 | tf_op jit(solution)/shard_map/stack | solution.py:13
  8.9 1.7 %all-to-all-done = bf16[1,128,4,128]{3,1,0,2:T(8,128)(2,1)S(1)} async-done(((bf16[1,128,4,128]{3,1,0,2:T(8,128)(2,1)}), bf16[1,128,4,128]{3,1,0,2:T(8,128)(2,1)S(1)}, u32[]{:S(2)}, u32[]{:S(2)}) %all-to-all-start) | async-done | bytes 131104 | tf_op jit(solution)/shard_map/all_to_all | solution.py:57
  10.6 3.3 %all-to-all-start.1 = ((bf16[1,128,4,128]{3,1,0,2:T(8,128)(2,1)}), bf16[1,128,4,128]{3,1,0,2:T(8,128)(2,1)S(1)}, u32[]{:S(2)}, u32[]{:S(2)}) async-start(bf16[1,128,4,128]{3,1,0,2:T(8,128)(2,1)} %copy.35), calls=%async_computation.1 | async-start | bytes 262144 | tf_op jit(solution)/shard_map/all_to_all | solution.py:58
  13.9 4.6 %all-to-all-done.1 = bf16[1,128,4,128]{3,1,0,2:T(8,128)(2,1)S(1)} async-done(((bf16[1,128,4,128]{3,1,0,2:T(8,128)(2,1)}), bf16[1,128,4,128]{3,1,0,2:T(8,128)(2,1)S(1)}, u32[]{:S(2)}, u32[]{:S(2)}) %all-to-all-start.1) | async-done | bytes 131104 | tf_op jit(solution)/shard_map/all_to_all | solution.py:58
  18.5 3.3 %all-to-all-start.2 = ((bf16[4,1,128,1,128]{4,2,3,1,0:T(8,128)(2,1)}), bf16[4,1,128,1,128]{4,2,3,1,0:T(8,128)(2,1)S(1)}, u32[]{:S(2)}, u32[]{:S(2)}) async-start(bf16[4,1,128,1,128]{4,2,3,1,0:T(8,128)(2,1)} %pad_maximum_fusion), calls=%async_computation.2 | async-start | bytes 262144 | tf_op jit(solution)/shard_map/all_to_all | solution.py:13
  21.8 0.4 %fusion.9 = (f32[512]{0:T(512)S(1)}, f32[512,512]{0,1:T(8,128)S(1)}) fusion(bf16[1,512,1,128]{3,1,2,0:T(8,128)(2,1)S(1)} %bitcast.63, bf16[1,512,1,128]{3,1,2,0:T(8,128)(2,1)S(1)} %bitcast.59, s32[512]{0:T(512)S(1)} %add_select_fusion), kind=kOutput, calls=%fused_computation.33 | convolution fusion | flops 34602496 | bytes 1316864 | tf_op jit(solution)/shard_map/while/body/eval_jaxpr/while/body/eval_jaxpr/dot_general | solution.py:26
  22.2 0.3 fusion.10
  22.5 0.2 fusion.3
  22.7 0.2 fusion.2
  22.9 3.5 %all-to-all-done.2 = bf16[4,1,128,1,128]{4,2,3,1,0:T(8,128)(2,1)S(1)} async-done(((bf16[4,1,128,1,128]{4,2,3,1,0:T(8,128)(2,1)}), bf16[4,1,128,1,128]{4,2,3,1,0:T(8,128)(2,1)S(1)}, u32[]{:S(2)}, u32[]{:S(2)}) %all-to-all-start.2) | async-done | bytes 131104 | tf_op jit(solution)/shard_map/all_to_all | solution.py:13
  26.4 0.3 convolution_multiply_fusion.2
  26.7 0.4 multiply_reduce_fusion
  27.1 0.0 copy-start.2
  27.1 0.6 %copy-done.2 = f32[128]{0:T(128)S(1)} copy-done((f32[128]{0:T(128)S(1)}, f32[128]{0:T(128)}, u32[]{:S(2)}) %copy-start.2) | copy-done | bytes 536
  27.8 0.1 fusion.4
  27.8 0.2 copy.43
  28.0 0.5 %broadcast.100 = bf16[]{:T(256)} broadcast(bf16[]{:T(256)} %constant.141), dimensions={} | broadcast | bytes 4
  28.5 1.4 %reduce.2 = bf16[512,128]{1,0:T(8,128)(2,1)S(1)} reduce(bf16[512,1,1,128]{3,2,1,0:T(2,128)(2,1)S(1)} %bitcast.56, bf16[]{:T(256)} %broadcast.100), dimensions={1,2}, to_apply=%bitcast.43.reduce_sub_computation | reduce | bytes 262146
  30.0 7.0 %all_to_all.59 = bf16[4,2,8192]{2,1,0:T(2,128)(2,1)S(1)} all-to-all(bf16[4,2,8192]{2,1,0:T(2,128)(2,1)S(1)} %reshape.63), channel_id=1, replica_groups=mesh['sp'=4,'dp'=8] {'sp'}, dimensions={0} | all-to-all | bytes 262144 | tf_op jit(solution)/shard_map/all_to_all | solution.py:64
  37.0 0.1 reshape.64
  37.1 0.8 %copy.44 = bf16[1,128,4,128]{3,2,1,0:T(4,128)(2,1)} copy(bf16[1,128,4,128]{3,1,2,0:T(8,128)(2,1)S(1)} %bitcast.58) | data formatting | bytes 262144 | tf_op jit(solution)/shard_map/all_to_all | solution.py:64
  (6 shorter events, 0.1 us)
Async XLA Ops:
  1.6 4.4 %copy-start = (bf16[1,128,4,128]{3,2,1,0:T(4,128)(2,1)S(1)}, bf16[1,128,4,128]{3,2,1,0:T(4,128)(2,1)}, u32[]{:S(2)}) copy-start(bf16[1,128,4,128]{3,2,1,0:T(4,128)(2,1)} %param.7) | copy-start | bytes 393220
  1.6 9.0 %all-to-all-start = ((bf16[1,128,4,128]{3,1,0,2:T(8,128)(2,1)}), bf16[1,128,4,128]{3,1,0,2:T(8,128)(2,1)S(1)}, u32[]{:S(2)}, u32[]{:S(2)}) async-start(bf16[1,128,4,128]{3,1,0,2:T(8,128)(2,1)} %copy.33), calls=%async_computation | async-start | bytes 262144 | tf_op jit(solution)/shard_map/all_to_all | solution.py:57
  6.0 0.9 %copy-start.1 = (bf16[1,128,4,128]{3,2,1,0:T(4,128)(2,1)S(1)}, bf16[1,128,4,128]{3,2,1,0:T(4,128)(2,1)}, u32[]{:S(2)}) copy-start(bf16[1,128,4,128]{3,2,1,0:T(4,128)(2,1)} %param.6) | copy-start | bytes 393220
  10.6 7.9 %all-to-all-start.1 = ((bf16[1,128,4,128]{3,1,0,2:T(8,128)(2,1)}), bf16[1,128,4,128]{3,1,0,2:T(8,128)(2,1)S(1)}, u32[]{:S(2)}, u32[]{:S(2)}) async-start(bf16[1,128,4,128]{3,1,0,2:T(8,128)(2,1)} %copy.35), calls=%async_computation.1 | async-start | bytes 262144 | tf_op jit(solution)/shard_map/all_to_all | solution.py:58
  18.5 7.9 %all-to-all-start.2 = ((bf16[4,1,128,1,128]{4,2,3,1,0:T(8,128)(2,1)}), bf16[4,1,128,1,128]{4,2,3,1,0:T(8,128)(2,1)S(1)}, u32[]{:S(2)}, u32[]{:S(2)}) async-start(bf16[4,1,128,1,128]{4,2,3,1,0:T(8,128)(2,1)} %pad_maximum_fusion), calls=%async_computation.2 | async-start | bytes 262144 | tf_op jit(solution)/shard_map/all_to_all | solution.py:13
  27.1 0.7 %copy-start.2 = (f32[128]{0:T(128)S(1)}, f32[128]{0:T(128)}, u32[]{:S(2)}) copy-start(f32[128]{0:T(128)} %param.9) | copy-start | bytes 1540
